TPU v7x, 32 devices: a whole 2x2x4 slice. The times are simulated.
32 devices in a mesh: sp: 16 (over z, y, x), tp: 2 (over core).
Axes of the slice: x: 2, y: 2, z: 4, core: 2. Of those that a mesh axis runs over, the one named last changes fastest.
Arguments:
- tokens: bfloat16 [4096, 2048], P('sp'), may hold values from -6 to 6
- input_norm_gain: float32 [2048], replicated, may hold values from 0.1 to 1.9
- query_matrix: bfloat16 [2048, 1024], P('sp', 'tp'), may hold values from -0.125 to 0.125
- key_matrix: bfloat16 [2048, 1024], P('sp', 'tp'), may hold values from -0.125 to 0.125
- value_matrix: bfloat16 [2048, 1024], P('sp', 'tp'), may hold values from -0.125 to 0.125
- convolution_value_matrix: bfloat16 [2048, 2048], P('sp', 'tp'), may hold values from -0.125 to 0.125
- convolution_gate_matrix: bfloat16 [2048, 2048], P('sp', 'tp'), may hold values from -0.125 to 0.125
- decay_offset_channel: float32 [1024], P('tp'), may hold values from -16 to -2
- decay_first_matrix: bfloat16 [2048, 128], replicated, may hold values from -0.125 to 0.125
- decay_second_matrix: bfloat16 [128, 1024], P(None, 'tp'), may hold values from -0.59765625 to 0.59765625
- learning_rate_offset: float32 [1024], P('tp'), may hold values from -9 to 1
- learning_rate_first_matrix: bfloat16 [2048, 128], replicated, may hold values from -0.125 to 0.125
- learning_rate_second_matrix: bfloat16 [128, 1024], P(None, 'tp'), may hold values from -0.5 to 0.5
- forgetting_rate_factor: float32 [4096, 16], P('sp', 'tp'), may hold values from 0.39 to 2.53
- state_retention_share: float32 [4096, 16], P('sp', 'tp'), may hold values from 0.12 to 1
- per_head_norm_gain: float32 [1024], P('tp'), may hold values from 0.1 to 1.9
- convolution_filter_taps: float32 [31, 2048], P(None, 'tp'), may hold values from -81 to 81
- convolution_channel_gain: float32 [2048], P('tp'), may hold values from 0.1 to 1.9
- attention_output_matrix: bfloat16 [2048, 1024], P('sp', 'tp'), may hold values from -0.109375 to 0.109375
- convolution_output_matrix: bfloat16 [2048, 2048], P('sp', 'tp'), may hold values from -0.109375 to 0.109375
Outputs:
- mixed: bfloat16 [4096, 2048], P('sp')
All inputs are finite; a program needn't handle non-finite values.
Results may differ from a plain program's by a relative error of at most 0.014.
Values may be sent and summed in bfloat16 or wider, within the bound.
A program may use at most 128 MiB of HBM per device.

v0:
```python
import math
import jax
import jax.numpy as jnp
from jax import lax
from jax.sharding import PartitionSpec as P

CONV_CH = 2048
HIGHEST = lax.Precision.HIGHEST
RMS_EPSILON = 1e-06
GROUP_EPSILON = 0.00064
LAYER_EPSILON = 1e-05
UNIT_EPSILON = 1e-06


def entering(x, axis, combine, identity):
    count, place = (lax.axis_size(axis), lax.axis_index(axis))
    everything = jax.tree.map(lambda part: lax.all_gather(part, axis), x)
    start = jax.tree.map(
        lambda part, zero: jnp.broadcast_to(jnp.asarray(zero, part.dtype), part.shape), x, identity
    )

    def hop(k, before):
        reached = k < place
        new = combine(before, jax.tree.map(lambda part: part[k], everything))
        return jax.tree.map(lambda a, b: jnp.where(reached, a, b), new, before)

    return lax.fori_loop(0, count, hop, start)


def from_behind(value, axis, steps):
    count = lax.axis_size(axis)
    initial, last = (max(0, -steps), min(count, count - steps))
    return lax.ppermute(value, axis, [(source, source + steps) for source in range(initial, last)])


def exact_mul(form, left, right):
    return jnp.einsum(form, left, right, precision=HIGHEST)


def chain_pair(earlier, later):
    return (
        exact_mul("...cd,...de->...ce", earlier[0], later[0]),
        exact_mul("...vd,...de->...ve", earlier[1], later[0]) + later[1],
    )


def split_blocks(values, block_count, block_len):
    return values.reshape((block_count, block_len) + values.shape[1:]).transpose(0, 2, 1, 3)


def block_update(carry, inputs):
    phi_sofar, psi_sofar = carry
    query_blk, logdec_blk, key_blk, value_blk, erase_blk, write_blk = inputs
    block_len = query_blk.shape[1]
    head_size = query_blk.shape[2]
    log_gain = jnp.cumsum(logdec_blk, axis=1)
    log_before = log_gain - logdec_blk
    positions = jnp.arange(block_len)
    strict = positions[:, None] > positions[None, :]
    pair_decay = jnp.exp(
        jnp.where(
            strict[None, :, :, None], log_before[:, :, None, :] - log_gain[:, None, :, :], -jnp.inf
        )
    )

    def paired(left, right):
        return jnp.einsum("htc,htsc,hsc->hts", left, pair_decay, right, precision=HIGHEST)

    step_query = query_blk * jnp.exp(logdec_blk)
    identity_blk = jnp.eye(block_len, dtype=jnp.float32)
    erase_write = paired(erase_blk, write_blk)
    erase_key = paired(erase_blk, key_blk)
    read_write = (
        paired(step_query, write_blk)
        + identity_blk * jnp.sum(query_blk * write_blk, axis=-1)[:, :, None]
    )
    read_key = (
        paired(step_query, key_blk)
        + identity_blk * jnp.sum(query_blk * key_blk, axis=-1)[:, :, None]
    )
    inverse = identity_blk + erase_write
    power = erase_write
    for level in range(block_len.bit_length() - 2):
        power = exact_mul("hts,hsu->htu", power, power)
        inverse = inverse + exact_mul("hts,hsu->htu", inverse, power)
    erase_hat = erase_blk * jnp.exp(log_before)
    query_hat = query_blk * jnp.exp(log_gain)
    total_gain = log_gain[:, -1:, :]
    to_end = jnp.exp(total_gain - log_gain)
    write_end = write_blk * to_end
    key_end = key_blk * to_end
    pulled = exact_mul("hts,hsv->htv", inverse, exact_mul("hts,hsv->htv", erase_key, value_blk))
    local_out = exact_mul("hts,hsv->htv", read_write, pulled) + exact_mul(
        "hts,hsv->htv", read_key, value_blk
    )
    psi_block = exact_mul("hsv,hsc->hvc", pulled, write_end) + exact_mul(
        "hsv,hsc->hvc", value_blk, key_end
    )
    erase_solved = exact_mul("hts,hsc->htc", inverse, erase_hat)
    query_full = query_hat + exact_mul("hts,hsc->htc", read_write, erase_solved)
    identity_key = jnp.eye(head_size, dtype=jnp.float32)
    phi_block = jnp.exp(total_gain[:, 0, :])[:, :, None] * identity_key + exact_mul(
        "hsc,hsd->hcd", erase_solved, write_end
    )
    local_out = local_out + exact_mul("htc,hvc->htv", query_full, psi_sofar)
    carried_query = exact_mul("htc,hdc->htd", query_full, phi_sofar)
    phi_next = exact_mul("hcd,hde->hce", phi_sofar, phi_block)
    psi_next = exact_mul("hvd,hde->hve", psi_sofar, phi_block) + psi_block
    return ((phi_next, psi_next), (local_out, carried_query))


def body(
    tokens,
    input_norm_gain,
    query_matrix,
    key_matrix,
    value_matrix,
    convolution_value_matrix,
    convolution_gate_matrix,
    decay_offset_channel,
    decay_first_matrix,
    decay_second_matrix,
    learning_rate_offset,
    learning_rate_first_matrix,
    learning_rate_second_matrix,
    forgetting_rate_factor,
    state_retention_share,
    per_head_norm_gain,
    convolution_filter_taps,
    convolution_channel_gain,
    attention_output_matrix,
    convolution_output_matrix,
):
    tok_rows = tokens.shape[0]
    heads_dev = forgetting_rate_factor.shape[1]
    head_size = query_matrix.shape[1] // heads_dev
    widened = tokens.astype(jnp.float32)
    normed = (
        widened
        * lax.rsqrt(jnp.mean(widened * widened, axis=-1, keepdims=True) + RMS_EPSILON)
        * input_norm_gain
    ).astype(jnp.bfloat16)
    pieces = (
        lax.all_gather(query_matrix, "sp", axis=0, tiled=True),
        lax.all_gather(key_matrix, "sp", axis=0, tiled=True),
        lax.all_gather(value_matrix, "sp", axis=0, tiled=True),
        lax.all_gather(convolution_value_matrix, "sp", axis=0, tiled=True),
        lax.all_gather(convolution_gate_matrix, "sp", axis=0, tiled=True),
    )
    query_proj, key_proj, value_proj, conv_value, conv_gate = tuple(
        (jnp.dot(normed, piece, preferred_element_type=jnp.float32) for piece in pieces)
    )
    decay_mid = jnp.tanh(
        jnp.dot(normed, decay_first_matrix, preferred_element_type=jnp.float32)
    ).astype(jnp.bfloat16)
    rate_mid = jnp.dot(
        normed, learning_rate_first_matrix, preferred_element_type=jnp.float32
    ).astype(jnp.bfloat16)
    logarithm_learning_rate = (
        -jax.nn.softplus(
            -(
                decay_offset_channel
                + jnp.dot(decay_mid, decay_second_matrix, preferred_element_type=jnp.float32)
            )
        )
        - 0.5
    )
    learn_rate = jax.nn.sigmoid(
        learning_rate_offset
        + jnp.dot(rate_mid, learning_rate_second_matrix, preferred_element_type=jnp.float32)
    )
    reshaped_tensor = (tok_rows, heads_dev, head_size)
    log_decay = (
        -jnp.exp(logarithm_learning_rate).reshape(reshaped_tensor)
        * forgetting_rate_factor[:, :, None]
        + jnp.log(state_retention_share)[:, :, None]
    )
    key_heads = key_proj.reshape(reshaped_tensor)
    unit_key = key_heads * lax.rsqrt(
        jnp.sum(key_heads * key_heads, axis=-1, keepdims=True) + UNIT_EPSILON
    )
    erase = -unit_key
    write = unit_key * learn_rate.reshape(reshaped_tensor)
    block_len = math.gcd(tok_rows, 128)
    block_count = tok_rows // block_len
    inputs = tuple(
        (
            split_blocks(item, block_count, block_len)
            for item in (
                query_proj.reshape(reshaped_tensor),
                log_decay,
                key_heads,
                value_proj.reshape(reshaped_tensor),
                erase,
                write,
            )
        )
    )
    identity_key = jnp.broadcast_to(
        jnp.eye(head_size, dtype=jnp.float32), (heads_dev, head_size, head_size)
    )
    device_pair, block_outs = lax.scan(
        block_update, (identity_key, jnp.zeros_like(identity_key)), inputs
    )
    local_out, carried_query = block_outs
    phi_device, psi_device = device_pair
    prefix = entering(
        (phi_device, psi_device), "sp", chain_pair, (identity_key, jnp.zeros_like(identity_key))
    )
    state_in = prefix[1]
    state_out = local_out + exact_mul("bhtd,hvd->bhtv", carried_query, state_in)
    state_rows = state_out.transpose(0, 2, 1, 3).reshape(reshaped_tensor)
    centred = state_rows - jnp.mean(state_rows, axis=-1, keepdims=True)
    normal_state = centred * lax.rsqrt(
        jnp.mean(centred * centred, axis=-1, keepdims=True) + GROUP_EPSILON
    )
    state_mixed = (
        (normal_state * per_head_norm_gain.reshape(heads_dev, head_size))
        .reshape(tok_rows, heads_dev * head_size)
        .astype(jnp.bfloat16)
    )
    gated = (conv_value * jax.nn.sigmoid(conv_gate)).astype(jnp.bfloat16)
    span = convolution_filter_taps.shape[0]
    rim = from_behind(gated[tok_rows - (span - 1) :], "sp", 1)
    padded = jnp.concatenate([rim, gated], axis=0)
    filtered = jnp.zeros(gated.shape, jnp.float32)
    for offset in range(span):
        filtered = filtered + convolution_filter_taps[offset] * padded[offset : offset + tok_rows]
    total_sum, total_square = lax.psum(
        (jnp.sum(filtered, axis=-1), jnp.sum(filtered * filtered, axis=-1)), "tp"
    )
    row_mean = total_sum / CONV_CH
    deviation = filtered - row_mean[:, None]
    variance = total_square / CONV_CH - row_mean * row_mean
    conv_mixed = jax.nn.silu(
        deviation * lax.rsqrt(variance + LAYER_EPSILON)[:, None] * convolution_channel_gain
    ).astype(jnp.bfloat16)
    contract_dims = (((1,), (1,)), ((), ()))
    pieces = lax.all_gather(
        (attention_output_matrix, convolution_output_matrix), "sp", axis=0, tiled=True
    )
    partial_out = lax.dot_general(
        state_mixed, pieces[0], contract_dims, preferred_element_type=jnp.float32
    ) + lax.dot_general(conv_mixed, pieces[1], contract_dims, preferred_element_type=jnp.float32)
    return lax.psum(partial_out.astype(jnp.bfloat16), "tp")


def solution(mesh):
    return jax.shard_map(
        body,
        mesh=mesh,
        in_specs=(
            P("sp", None),
            P(),
            P("sp", "tp"),
            P("sp", "tp"),
            P("sp", "tp"),
            P("sp", "tp"),
            P("sp", "tp"),
            P("tp"),
            P(),
            P(None, "tp"),
            P("tp"),
            P(),
            P(None, "tp"),
            P("sp", "tp"),
            P("sp", "tp"),
            P("tp"),
            P(None, "tp"),
            P("tp"),
            P("sp", "tp"),
            P("sp", "tp"),
        ),
        out_specs=P("sp", None),
        check_vma=False,
    )
```

profile of v0, /device:TPU:0, one launch (start us, length us, event | category | flops | bytes accessed | tf_op | source)
XLA Modules:
  0.0 1069.4 jit_solution(5047170836986482139)
XLA Ops:
  17.3 55.9 %all-gather.12.cloned.1.call-done = bf16[2048,512]{1,0:T(8,128)(2,1)} async-done(((bf16[128,512]{1,0:T(8,128)(2,1)}), bf16[2048,512]{1,0:T(8,128)(2,1)}) %all-gather.12.cloned.1.call-update) | async-done | bytes 2097168 | tf_op jit(solution)/shard_map/all_gather | solution.py:145
  77.1 58.1 %all-gather.14.cloned.1.call-done = bf16[2048,512]{1,0:T(8,128)(2,1)} async-done(((bf16[128,512]{1,0:T(8,128)(2,1)}), bf16[2048,512]{1,0:T(8,128)(2,1)}) %all-gather.14.cloned.1.call-update) | async-done | bytes 2097168 | tf_op jit(solution)/shard_map/all_gather | solution.py:146
  138.1 59.1 %all-gather.16.cloned.1.call-done = bf16[2048,512]{1,0:T(8,128)(2,1)} async-done(((bf16[128,512]{1,0:T(8,128)(2,1)}), bf16[2048,512]{1,0:T(8,128)(2,1)}) %all-gather.16.cloned.1.call-update) | async-done | bytes 2097168 | tf_op jit(solution)/shard_map/all_gather | solution.py:144
  204.2 387.9 %while.31 = (s32[]{:T(128)}, f32[8,64,64]{1,2,0:T(8,128)}, f32[8,64,64]{1,2,0:T(8,128)S(1)}, f32[2,8,128,64]{2,3,0,1:T(8,128)}, f32[2,8,128,64]{2,3,0,1:T(8,128)...) while((s32[]{:T(128)}, f32[8,64,64]{1,2,0:T(8,128)}, ...), condition=%wide.region_6.7_spmd.clone, body=%wide.region_2.6_spmd.clone.sunk | while | flops 3836598272 | bytes 58414024 | solution.py:202
  206.6 23.3 %fusion.369 = f32[8,128,64]{2,0,1:T(8,128)S(1)} fusion(f32[8,128,64]{2,0,1:T(8,128)S(1)} %copy.214), kind=kOutput, calls=%fused_computation.245.clone.1 | output fusion | flops 8323072 | bytes 524288 | tf_op jit(solution)/shard_map/while/body/eval_jaxpr/jit(cumsum)/reduce_window_sum | solution.py:56
  235.5 33.2 %fusion.370 = f32[8,128,1,128]{3,2,1,0:T(1,128)S(1)} fusion(f32[8,128,64,1]{2,3,1,0:T(1,128)} %copy.213, f32[8,128,64]{1,2,0:T(8,128)S(1)} %bitcast.376, f32[8,128,64]{1,2,0:T(8,128)S(1)} %copy.215, f32[8,128,64]{2,1,0:T(8,128)S(1)} %copy.216, pred[128,128]{1,0:T(8,128)(4,1)S(1)} %iota_compare_fusion.5), kind=kOutput, calls=%fused_computation.6.clone.1 | convolution fusion | flops 125829120 | bytes 1589248 | tf_op jit(solution)/shard_map/while/body/eval_jaxpr/htc,htsc,hsc->hts/dot_general | solution.py:67
  276.7 35.6 %fusion.381 = f32[8,128,1,128]{3,2,1,0:T(1,128)S(1)} fusion(f32[8,128,64,1]{2,3,1,0:T(1,128)S(1)} %copy-done.6, f32[8,128,64]{1,2,0:T(8,128)S(1)} %bitcast.390, f32[8,128,64]{1,2,0:T(8,128)S(1)} %copy.215, f32[8,128,64]{2,1,0:T(8,128)S(1)} %copy-done.4, pred[128,128]{1,0:T(8,128)(4,1)S(1)} %iota_compare_fusion.5), kind=kOutput, calls=%fused_computation.2.clone.1 | convolution fusion | flops 125829120 | bytes 1589248 | tf_op jit(solution)/shard_map/while/body/eval_jaxpr/htc,htsc,hsc->hts/dot_general | solution.py:67
  317.8 33.1 %fusion.386 = f32[8,128,1,128]{3,2,1,0:T(1,128)S(1)} fusion(f32[8,128,64,1]{2,3,1,0:T(1,128)} %copy.217, f32[8,128,64]{1,2,0:T(8,128)S(1)} %bitcast.378, f32[8,128,64]{1,2,0:T(8,128)S(1)} %copy.215, f32[8,128,64]{2,1,0:T(8,128)} %copy-done.3, pred[128,128]{1,0:T(8,128)(4,1)S(1)} %iota_compare_fusion.5), kind=kOutput, calls=%fused_computation.4.clone.1 | convolution fusion | flops 125829120 | bytes 1589248 | tf_op jit(solution)/shard_map/while/body/eval_jaxpr/htc,htsc,hsc->hts/dot_general | solution.py:67
  352.0 31.7 %fusion.388 = f32[8,128,1,128]{3,2,1,0:T(1,128)S(1)} fusion(f32[8,128,64,1]{2,3,1,0:T(1,128)S(1)} %copy-done.7, f32[8,128,64]{1,2,0:T(8,128)S(1)} %bitcast.391, f32[8,128,64]{1,2,0:T(8,128)S(1)} %copy.215, f32[8,128,64]{2,1,0:T(8,128)S(1)} %copy-done.5, pred[128,128]{1,0:T(8,128)(4,1)S(1)} %iota_compare_fusion.5), kind=kOutput, calls=%fused_computation.clone.2 | convolution fusion | flops 125829120 | bytes 1589248 | tf_op jit(solution)/shard_map/while/body/eval_jaxpr/htc,htsc,hsc->hts/dot_general | solution.py:67
  397.4 23.3 %fusion.369 = f32[8,128,64]{2,0,1:T(8,128)S(1)} fusion(f32[8,128,64]{2,0,1:T(8,128)S(1)} %copy.214), kind=kOutput, calls=%fused_computation.245.clone.1 | output fusion | flops 8323072 | bytes 524288 | tf_op jit(solution)/shard_map/while/body/eval_jaxpr/jit(cumsum)/reduce_window_sum | solution.py:56
  426.4 33.0 %fusion.370 = f32[8,128,1,128]{3,2,1,0:T(1,128)S(1)} fusion(f32[8,128,64,1]{2,3,1,0:T(1,128)} %copy.213, f32[8,128,64]{1,2,0:T(8,128)S(1)} %bitcast.376, f32[8,128,64]{1,2,0:T(8,128)S(1)} %copy.215, f32[8,128,64]{2,1,0:T(8,128)S(1)} %copy.216, pred[128,128]{1,0:T(8,128)(4,1)S(1)} %iota_compare_fusion.5), kind=kOutput, calls=%fused_computation.6.clone.1 | convolution fusion | flops 125829120 | bytes 1589248 | tf_op jit(solution)/shard_map/while/body/eval_jaxpr/htc,htsc,hsc->hts/dot_general | solution.py:67
  467.4 35.6 %fusion.381 = f32[8,128,1,128]{3,2,1,0:T(1,128)S(1)} fusion(f32[8,128,64,1]{2,3,1,0:T(1,128)S(1)} %copy-done.6, f32[8,128,64]{1,2,0:T(8,128)S(1)} %bitcast.390, f32[8,128,64]{1,2,0:T(8,128)S(1)} %copy.215, f32[8,128,64]{2,1,0:T(8,128)S(1)} %copy-done.4, pred[128,128]{1,0:T(8,128)(4,1)S(1)} %iota_compare_fusion.5), kind=kOutput, calls=%fused_computation.2.clone.1 | convolution fusion | flops 125829120 | bytes 1589248 | tf_op jit(solution)/shard_map/while/body/eval_jaxpr/htc,htsc,hsc->hts/dot_general | solution.py:67
  508.5 33.1 %fusion.386 = f32[8,128,1,128]{3,2,1,0:T(1,128)S(1)} fusion(f32[8,128,64,1]{2,3,1,0:T(1,128)} %copy.217, f32[8,128,64]{1,2,0:T(8,128)S(1)} %bitcast.378, f32[8,128,64]{1,2,0:T(8,128)S(1)} %copy.215, f32[8,128,64]{2,1,0:T(8,128)} %copy-done.3, pred[128,128]{1,0:T(8,128)(4,1)S(1)} %iota_compare_fusion.5), kind=kOutput, calls=%fused_computation.4.clone.1 | convolution fusion | flops 125829120 | bytes 1589248 | tf_op jit(solution)/shard_map/while/body/eval_jaxpr/htc,htsc,hsc->hts/dot_general | solution.py:67
  542.7 31.7 %fusion.388 = f32[8,128,1,128]{3,2,1,0:T(1,128)S(1)} fusion(f32[8,128,64,1]{2,3,1,0:T(1,128)S(1)} %copy-done.7, f32[8,128,64]{1,2,0:T(8,128)S(1)} %bitcast.391, f32[8,128,64]{1,2,0:T(8,128)S(1)} %copy.215, f32[8,128,64]{2,1,0:T(8,128)S(1)} %copy-done.5, pred[128,128]{1,0:T(8,128)(4,1)S(1)} %iota_compare_fusion.5), kind=kOutput, calls=%fused_computation.clone.2 | convolution fusion | flops 125829120 | bytes 1589248 | tf_op jit(solution)/shard_map/while/body/eval_jaxpr/htc,htsc,hsc->hts/dot_general | solution.py:67
  597.9 70.6 %all-gather.26.cloned.1.call-done = f32[128,64,64]{2,1,0:T(8,128)} async-done(((f32[8,64,64]{2,1,0:T(8,128)}), f32[128,64,64]{2,1,0:T(8,128)}) %all-gather.26.cloned.1.call-update) | async-done | bytes 2097168 | tf_op jit(solution)/shard_map/all_gather | solution.py:17
  668.5 76.8 %all-gather.28.cloned.1.call-done = f32[128,64,64]{2,1,0:T(8,128)} async-done(((f32[8,64,64]{2,1,0:T(8,128)}), f32[128,64,64]{2,1,0:T(8,128)}) %all-gather.28.cloned.1.call-update) | async-done | bytes 2097168 | tf_op jit(solution)/shard_map/all_gather | solution.py:17
  745.4 43.6 %while.32 = (s32[]{:T(128)}, f32[8,64,64]{1,2,0:T(8,128)S(1)}, s32[]{:T(128)}, f32[16,8,64,64]{3,2,1,0:T(8,128)}, f32[16,8,64,64]{3,2,1,0:T(8,128)}, /*index=5*/s32[]{:T(128)}, s32[]{:T(128)}) while((s32[]{:T(128)}, f32[8,64,64]{1,2,0:T(8,128)S(1)}, s32[]{:T(128)}, f32[16,8,64,64]{3,2,1,0:T(8,128)}, f32[16,8,64,64]{3,2,1,0:T(8,128)}, ...), condition=%wide.region_8.9_spmd.clone, body=%wide.region_7.8_spmd.clone.sunk | while | flops 25296900 | bytes 1968227 | solution.py:27
  789.0 33.2 %all-gather.22.cloned.1.call-done = bf16[2048,1024]{1,0:T(8,128)(2,1)} async-done(((bf16[128,1024]{1,0:T(8,128)(2,1)}), bf16[2048,1024]{1,0:T(8,128)(2,1)}) %all-gather.22.cloned.1.call-update) | async-done | bytes 4194320 | tf_op jit(solution)/shard_map/all_gather | solution.py:148
  822.2 4.5 fusion.88
  826.8 72.4 %all-gather.20.cloned.1.call-done = bf16[2048,1024]{1,0:T(8,128)(2,1)} async-done(((bf16[128,1024]{1,0:T(8,128)(2,1)}), bf16[2048,1024]{1,0:T(8,128)(2,1)}) %all-gather.20.cloned.1.call-update) | async-done | bytes 4194320 | tf_op jit(solution)/shard_map/all_gather | solution.py:147
  908.3 6.0 fusion.155
  916.7 59.5 %all-gather.24.cloned.1.call-done = bf16[2048,1024]{1,0:T(8,128)(2,1)} async-done(((bf16[128,1024]{1,0:T(8,128)(2,1)}), bf16[2048,1024]{1,0:T(8,128)(2,1)}) %all-gather.24.cloned.1.call-update) | async-done | bytes 4194320 | tf_op jit(solution)/shard_map/all_gather | solution.py:239
  980.2 57.8 %all-gather.18.cloned.1.call-done = bf16[2048,512]{1,0:T(8,128)(2,1)} async-done(((bf16[128,512]{1,0:T(8,128)(2,1)}), bf16[2048,512]{1,0:T(8,128)(2,1)}) %all-gather.18.cloned.1.call-update) | async-done | bytes 2097168 | tf_op jit(solution)/shard_map/all_gather | solution.py:239
  1041.4 18.4 %all-reduce.3.cloned.1.call-done = bf16[256,2048]{1,0:T(8,128)(2,1)} async-done(((bf16[256,2048]{1,0:T(8,128)(2,1)}), bf16[256,2048]{1,0:T(8,128)(2,1)}) %all-reduce.3.cloned.1.call-update) | async-done | bytes 1048592 | tf_op jit(solution)/shard_map/psum | solution.py:245
  (292 shorter events, 160.3 us)
Async XLA Ops:
  6.5 66.7 %all-gather.12.cloned.1.call-start = ((), (), s32[]{:S(2)}) async-start(), calls=%async_computation | async-start | bytes 2228224 | tf_op jit(solution)/shard_map/all_gather | solution.py:145
  7.3 128.0 %all-gather.14.cloned.1.call-start = ((), (), s32[]{:S(2)}) async-start(), calls=%async_computation.1 | async-start | bytes 2228224 | tf_op jit(solution)/shard_map/all_gather | solution.py:146
  8.0 189.2 %all-gather.16.cloned.1.call-start = ((), (), s32[]{:S(2)}) async-start(), calls=%async_computation.2 | async-start | bytes 2228224 | tf_op jit(solution)/shard_map/all_gather | solution.py:144
  8.7 659.8 %all-gather.26.cloned.1.call-start = ((), (), s32[]{:S(2)}) async-start(), calls=%async_computation.8 | async-start | bytes 4456448 | tf_op jit(solution)/shard_map/all_gather | solution.py:17
  10.3 186.9 %copy-start.21 = (f32[256]{0:T(256)}, f32[256]{0:T(256)S(1)}, u32[]{:S(2)}) copy-start(f32[256]{0:T(256)S(1)} %add_rsqrt_fusion.1) | copy-start | bytes 3076
  234.5 34.2 %copy-start.3 = (f32[8,128,64]{2,1,0:T(8,128)}, f32[8,128,64]{2,1,0:T(8,128)S(1)}, u32[]{:S(2)}) copy-start(f32[8,128,64]{2,1,0:T(8,128)S(1)} %copy.216) | copy-start | bytes 786436 | tf_op jit(solution)/shard_map/while
  317.8 34.3 %copy-start.5 = (f32[8,128,64]{2,1,0:T(8,128)S(1)}, f32[8,128,64]{2,1,0:T(8,128)}, u32[]{:S(2)}) copy-start(f32[8,128,64]{2,1,0:T(8,128)} %copy-done.3) | copy-start | bytes 786436 | tf_op jit(solution)/shard_map/while
  317.8 34.3 %copy-start.7 = (f32[8,128,64,1]{2,3,1,0:T(1,128)S(1)}, f32[8,128,64,1]{2,3,1,0:T(1,128)}, u32[]{:S(2)}) copy-start(f32[8,128,64,1]{2,3,1,0:T(1,128)} %copy.217) | copy-start | bytes 786436 | tf_op jit(solution)/shard_map/while
  425.3 34.0 %copy-start.3 = (f32[8,128,64]{2,1,0:T(8,128)}, f32[8,128,64]{2,1,0:T(8,128)S(1)}, u32[]{:S(2)}) copy-start(f32[8,128,64]{2,1,0:T(8,128)S(1)} %copy.216) | copy-start | bytes 786436 | tf_op jit(solution)/shard_map/while
  508.5 34.3 %copy-start.5 = (f32[8,128,64]{2,1,0:T(8,128)S(1)}, f32[8,128,64]{2,1,0:T(8,128)}, u32[]{:S(2)}) copy-start(f32[8,128,64]{2,1,0:T(8,128)} %copy-done.3) | copy-start | bytes 786436 | tf_op jit(solution)/shard_map/while
  508.5 34.3 %copy-start.7 = (f32[8,128,64,1]{2,3,1,0:T(1,128)S(1)}, f32[8,128,64,1]{2,3,1,0:T(1,128)}, u32[]{:S(2)}) copy-start(f32[8,128,64,1]{2,3,1,0:T(1,128)} %copy.217) | copy-start | bytes 786436 | tf_op jit(solution)/shard_map/while
  594.0 151.4 %all-gather.28.cloned.1.call-start = ((), (), s32[]{:S(2)}) async-start(), calls=%async_computation.9 | async-start | bytes 4456448 | tf_op jit(solution)/shard_map/all_gather | solution.py:17
  594.9 227.3 %all-gather.22.cloned.1.call-start = ((), (), s32[]{:S(2)}) async-start(), calls=%async_computation.5 | async-start | bytes 4456448 | tf_op jit(solution)/shard_map/all_gather | solution.py:148
  595.5 303.7 %all-gather.20.cloned.1.call-start = ((), (), s32[]{:S(2)}) async-start(), calls=%async_computation.4 | async-start | bytes 4456448 | tf_op jit(solution)/shard_map/all_gather | solution.py:147
  596.2 380.0 %all-gather.24.cloned.1.call-start = ((), (), s32[]{:S(2)}) async-start(), calls=%async_computation.6 | async-start | bytes 4456448 | tf_op jit(solution)/shard_map/all_gather | solution.py:239
  597.0 441.0 %all-gather.18.cloned.1.call-start = ((), (), s32[]{:S(2)}) async-start(), calls=%async_computation.3 | async-start | bytes 2228224 | tf_op jit(solution)/shard_map/all_gather | solution.py:239
  597.7 462.1 %all-reduce.3.cloned.1.call-start = ((), (), s32[]{:S(2)}) async-start(), calls=%async_computation.7 | async-start | bytes 2097152 | tf_op jit(solution)/shard_map/psum | solution.py:245
  745.4 76.9 %copy-start.12 = (bf16[256,2048]{1,0:T(8,128)(2,1)S(1)}, bf16[256,2048]{1,0:T(8,128)(2,1)}, u32[]{:S(2)}) copy-start(bf16[256,2048]{1,0:T(8,128)(2,1)} %param.24) | copy-start | bytes 3145732
  745.4 76.9 %copy-start.22 = (f32[256]{0:T(256)S(1)}, f32[256]{0:T(256)}, u32[]{:S(2)}) copy-start(f32[256]{0:T(256)} %copy-done.21) | copy-start | bytes 3076
  745.4 76.9 %copy-start.25 = (f32[2048]{0:T(1024)S(1)}, f32[2048]{0:T(1024)}, u32[]{:S(2)}) copy-start(f32[2048]{0:T(1024)} %param.25) | copy-start | bytes 24580
  826.8 79.6 %copy-start.13 = (f32[2,8,128,64]{2,3,0,1:T(8,128)S(1)}, f32[2,8,128,64]{2,3,0,1:T(8,128)}, u32[]{:S(2)}) copy-start(f32[2,8,128,64]{2,3,0,1:T(8,128)} %get-tuple-element.159) | copy-start | bytes 1572868
  826.8 79.6 %copy-start.16 = (f32[2,8,128,64]{2,3,0,1:T(8,128)S(1)}, f32[2,8,128,64]{2,3,0,1:T(8,128)}, u32[]{:S(2)}) copy-start(f32[2,8,128,64]{2,3,0,1:T(8,128)} %get-tuple-element.163) | copy-start | bytes 1572868
  903.0 5.2 collective-permute-start
  907.1 69.1 %copy-start.26 = (f32[1024]{0:T(1024)S(1)}, f32[1024]{0:T(1024)}, u32[]{:S(2)}) copy-start(f32[1024]{0:T(1024)} %param.41) | copy-start | bytes 12292
  (26 other events, 139.3 us)
Sparse Core Ops, SparseCore 0:
  10.1 63.0 all-gather.11
  76.0 59.1 all-gather.13
  138.0 59.1 all-gather.15
  594.1 74.3 all-gather.25
  671.1 74.1 all-gather.27
  748.0 74.1 all-gather.21
  825.0 74.1 all-gather.19
  902.0 74.1 all-gather.23
  979.0 58.9 all-gather.17
  1041.5 18.1 all-reduce.2
where the time goes:
time: 1080 us; the launch traced here: 1070 us
  waiting for transfers between devices  567 us (52%)
  matrix products  365 us (34%)
  other arithmetic  59.7 us (6%)
  local copies, waits for them, and re-layouts  48.4 us (4%)
  between operations  14.4 us (1%)
    dot_general x8, matrix products, paired(): jnp.einsum('htc,htsc,hsc->hts', left, pair_decay, right, precision=HIGHEST)  267 us
    all_gather x2, waiting for transfers between devices, entering(): everything = jax.tree.map(lambda part: lax.all_gather(part, axis), x)  147 us
    all_gather x2, waiting for transfers between devices, body(): lax.all_gather((attention_output_matrix, convolution_output_matrix), 'sp'...  117 us
    all_gather x1, waiting for transfers between devices, body(): lax.all_gather(convolution_value_matrix, 'sp', axis=0, tiled=True)  72.4 us
    dot_general x67, matrix products, exact_mul(): return jnp.einsum(form, left, right, precision=HIGHEST)  70.9 us
    all_gather x1, waiting for transfers between devices, body(): lax.all_gather(query_matrix, 'sp', axis=0, tiled=True)  59.1 us
    all_gather x1, waiting for transfers between devices, body(): lax.all_gather(value_matrix, 'sp', axis=0, tiled=True)  58.1 us
    all_gather x1, waiting for transfers between devices, body(): lax.all_gather(key_matrix, 'sp', axis=0, tiled=True)  55.9 us
  transfers between devices with their start and end apart: 11, of which 11 were waited for; matrix products, arithmetic and copies ran while one was open for 7% of the time, Pallas kernels for 0%

commit v1 on v0

--- a/solution.py
+++ b/solution.py
@@ -141,7 +141,9 @@
         * input_norm_gain
     ).astype(jnp.bfloat16)
     pieces = (
-        lax.all_gather(query_matrix, "sp", axis=0, tiled=True),
+        jnp.concatenate(
+            lax.all_to_all(jnp.stack([query_matrix] * lax.axis_size("sp")), "sp", 0, 0), axis=0
+        ),
         lax.all_gather(key_matrix, "sp", axis=0, tiled=True),
         lax.all_gather(value_matrix, "sp", axis=0, tiled=True),
         lax.all_gather(convolution_value_matrix, "sp", axis=0, tiled=True),

time: 1080 us -> 1030 us (0.954)
  waiting for transfers between devices: 567 us -> 499 us
    all_gather x1 -> x0, waiting for transfers between devices: 59.1 us -> none  [body(): lax.all_gather(query_matrix, 'sp', axis=0, tiled=True)]
  transfers between devices with their start and end apart: 11 -> 11, of which waited for: 11 -> 10; matrix products, arithmetic and copies ran while one was open for 7% -> 9% of each run, Pallas kernels for 0% -> 0%
where the time goes in v1:
time: 1030 us
  waiting for transfers between devices  499 us (48%)
  matrix products  369 us (36%)
  other arithmetic  62.7 us (6%)
  local copies, waits for them, and re-layouts  58.3 us (6%)
  between operations  13.8 us (1%)
  starting transfers between devices  12.1 us (1%)
    dot_general x8, matrix products, paired(): jnp.einsum('htc,htsc,hsc->hts', left, pair_decay, right, precision=HIGHEST)  267 us
    all_gather x2, waiting for transfers between devices, entering(): everything = jax.tree.map(lambda part: lax.all_gather(part, axis), x)  145 us
    all_gather x2, waiting for transfers between devices, body(): lax.all_gather((attention_output_matrix, convolution_output_matrix), 'sp'...  117 us
    dot_general x67, matrix products, exact_mul(): return jnp.einsum(form, left, right, precision=HIGHEST)  72.7 us
    all_gather x1, waiting for transfers between devices, body(): lax.all_gather(convolution_value_matrix, 'sp', axis=0, tiled=True)  72.3 us
    all_gather x1, waiting for transfers between devices, body(): lax.all_gather(key_matrix, 'sp', axis=0, tiled=True)  58.9 us
    all_gather x1, waiting for transfers between devices, body(): lax.all_gather(value_matrix, 'sp', axis=0, tiled=True)  49.5 us
    another operation x2, other arithmetic, block_update(): log_gain = jnp.cumsum(logdec_blk, axis=1)  46.6 us
  transfers between devices with their start and end apart: 11, of which 10 were waited for; matrix products, arithmetic and copies ran while one was open for 9% of the time, Pallas kernels for 0%

profile of v1, /device:TPU:0, one launch (start us, length us, event | category | flops | bytes accessed | tf_op | source)
XLA Modules:
  0.0 1025.8 jit_solution(3166189606075823311)
XLA Ops:
  10.0 8.5 all-to-all-start
  30.5 58.9 %all-gather.11.cloned.1.call-done = bf16[2048,512]{1,0:T(8,128)(2,1)} async-done(((bf16[128,512]{1,0:T(8,128)(2,1)}), bf16[2048,512]{1,0:T(8,128)(2,1)}) %all-gather.11.cloned.1.call-update) | async-done | bytes 2097168 | tf_op jit(solution)/shard_map/all_gather | solution.py:147
  102.1 49.5 %all-gather.13.cloned.1.call-done = bf16[2048,512]{1,0:T(8,128)(2,1)} async-done(((bf16[128,512]{1,0:T(8,128)(2,1)}), bf16[2048,512]{1,0:T(8,128)(2,1)}) %all-gather.13.cloned.1.call-update) | async-done | bytes 2097168 | tf_op jit(solution)/shard_map/all_gather | solution.py:148
  161.9 387.5 %while.31 = (s32[]{:T(128)}, f32[8,64,64]{1,2,0:T(8,128)}, f32[8,64,64]{1,2,0:T(8,128)S(1)}, f32[2,8,128,64]{2,3,0,1:T(8,128)}, f32[2,8,128,64]{2,3,0,1:T(8,128)...) while((s32[]{:T(128)}, f32[8,64,64]{1,2,0:T(8,128)}, ...), condition=%wide.region_6.7_spmd.clone, body=%wide.region_2.6_spmd.clone.sunk | while | flops 3836598272 | bytes 48321828 | solution.py:204
  163.4 23.3 %fusion.369 = f32[8,128,64]{2,0,1:T(8,128)S(1)} fusion(f32[8,128,64]{2,0,1:T(8,128)S(1)} %copy.253), kind=kOutput, calls=%fused_computation.246.clone.1 | output fusion | flops 8323072 | bytes 524288 | tf_op jit(solution)/shard_map/while/body/eval_jaxpr/jit(cumsum)/reduce_window_sum | solution.py:56
  192.8 32.8 %fusion.371 = f32[8,128,1,128]{3,2,1,0:T(1,128)S(1)} fusion(f32[8,128,64,1]{2,3,1,0:T(1,128)} %copy.252, f32[8,128,64]{1,2,0:T(8,128)S(1)} %bitcast.408, f32[8,128,64]{1,2,0:T(8,128)S(1)} %copy.254, f32[8,128,64]{2,1,0:T(8,128)S(1)} %copy.255, pred[128,128]{1,0:T(8,128)(4,1)S(1)} %iota_compare_fusion.5), kind=kOutput, calls=%fused_computation.6.clone.1 | convolution fusion | flops 125829120 | bytes 1589248 | tf_op jit(solution)/shard_map/while/body/eval_jaxpr/htc,htsc,hsc->hts/dot_general | solution.py:67
  233.6 35.6 %fusion.382 = f32[8,128,1,128]{3,2,1,0:T(1,128)S(1)} fusion(f32[8,128,64,1]{2,3,1,0:T(1,128)S(1)} %copy-done.5, f32[8,128,64]{1,2,0:T(8,128)S(1)} %bitcast.417, f32[8,128,64]{1,2,0:T(8,128)S(1)} %copy.254, f32[8,128,64]{2,1,0:T(8,128)S(1)} %copy-done.3, pred[128,128]{1,0:T(8,128)(4,1)S(1)} %iota_compare_fusion.5), kind=kOutput, calls=%fused_computation.2.clone.1 | convolution fusion | flops 125829120 | bytes 1589248 | tf_op jit(solution)/shard_map/while/body/eval_jaxpr/htc,htsc,hsc->hts/dot_general | solution.py:67
  273.8 33.0 %fusion.387 = f32[8,128,1,128]{3,2,1,0:T(1,128)S(1)} fusion(f32[8,128,64,1]{2,3,1,0:T(1,128)} %copy.256, f32[8,128,64]{1,2,0:T(8,128)S(1)} %bitcast.410, f32[8,128,64]{1,2,0:T(8,128)S(1)} %copy.254, f32[8,128,64]{2,1,0:T(8,128)} %copy-done.2, pred[128,128]{1,0:T(8,128)(4,1)S(1)} %iota_compare_fusion.5), kind=kOutput, calls=%fused_computation.4.clone.1 | convolution fusion | flops 125829120 | bytes 1589248 | tf_op jit(solution)/shard_map/while/body/eval_jaxpr/htc,htsc,hsc->hts/dot_general | solution.py:67
  308.1 31.9 %fusion.389 = f32[8,128,1,128]{3,2,1,0:T(1,128)S(1)} fusion(f32[8,128,64,1]{2,3,1,0:T(1,128)S(1)} %copy-done.6, f32[8,128,64]{1,2,0:T(8,128)S(1)} %bitcast.418, f32[8,128,64]{1,2,0:T(8,128)S(1)} %copy.254, f32[8,128,64]{2,1,0:T(8,128)S(1)} %copy-done.4, pred[128,128]{1,0:T(8,128)(4,1)S(1)} %iota_compare_fusion.5), kind=kOutput, calls=%fused_computation.clone.2 | convolution fusion | flops 125829120 | bytes 1589248 | tf_op jit(solution)/shard_map/while/body/eval_jaxpr/htc,htsc,hsc->hts/dot_general | solution.py:67
  354.0 23.3 %fusion.369 = f32[8,128,64]{2,0,1:T(8,128)S(1)} fusion(f32[8,128,64]{2,0,1:T(8,128)S(1)} %copy.253), kind=kOutput, calls=%fused_computation.246.clone.1 | output fusion | flops 8323072 | bytes 524288 | tf_op jit(solution)/shard_map/while/body/eval_jaxpr/jit(cumsum)/reduce_window_sum | solution.py:56
  383.4 32.8 %fusion.371 = f32[8,128,1,128]{3,2,1,0:T(1,128)S(1)} fusion(f32[8,128,64,1]{2,3,1,0:T(1,128)} %copy.252, f32[8,128,64]{1,2,0:T(8,128)S(1)} %bitcast.408, f32[8,128,64]{1,2,0:T(8,128)S(1)} %copy.254, f32[8,128,64]{2,1,0:T(8,128)S(1)} %copy.255, pred[128,128]{1,0:T(8,128)(4,1)S(1)} %iota_compare_fusion.5), kind=kOutput, calls=%fused_computation.6.clone.1 | convolution fusion | flops 125829120 | bytes 1589248 | tf_op jit(solution)/shard_map/while/body/eval_jaxpr/htc,htsc,hsc->hts/dot_general | solution.py:67
  424.2 35.6 %fusion.382 = f32[8,128,1,128]{3,2,1,0:T(1,128)S(1)} fusion(f32[8,128,64,1]{2,3,1,0:T(1,128)S(1)} %copy-done.5, f32[8,128,64]{1,2,0:T(8,128)S(1)} %bitcast.417, f32[8,128,64]{1,2,0:T(8,128)S(1)} %copy.254, f32[8,128,64]{2,1,0:T(8,128)S(1)} %copy-done.3, pred[128,128]{1,0:T(8,128)(4,1)S(1)} %iota_compare_fusion.5), kind=kOutput, calls=%fused_computation.2.clone.1 | convolution fusion | flops 125829120 | bytes 1589248 | tf_op jit(solution)/shard_map/while/body/eval_jaxpr/htc,htsc,hsc->hts/dot_general | solution.py:67
  464.4 33.0 %fusion.387 = f32[8,128,1,128]{3,2,1,0:T(1,128)S(1)} fusion(f32[8,128,64,1]{2,3,1,0:T(1,128)} %copy.256, f32[8,128,64]{1,2,0:T(8,128)S(1)} %bitcast.410, f32[8,128,64]{1,2,0:T(8,128)S(1)} %copy.254, f32[8,128,64]{2,1,0:T(8,128)} %copy-done.2, pred[128,128]{1,0:T(8,128)(4,1)S(1)} %iota_compare_fusion.5), kind=kOutput, calls=%fused_computation.4.clone.1 | convolution fusion | flops 125829120 | bytes 1589248 | tf_op jit(solution)/shard_map/while/body/eval_jaxpr/htc,htsc,hsc->hts/dot_general | solution.py:67
  498.6 31.9 %fusion.389 = f32[8,128,1,128]{3,2,1,0:T(1,128)S(1)} fusion(f32[8,128,64,1]{2,3,1,0:T(1,128)S(1)} %copy-done.6, f32[8,128,64]{1,2,0:T(8,128)S(1)} %bitcast.418, f32[8,128,64]{1,2,0:T(8,128)S(1)} %copy.254, f32[8,128,64]{2,1,0:T(8,128)S(1)} %copy-done.4, pred[128,128]{1,0:T(8,128)(4,1)S(1)} %iota_compare_fusion.5), kind=kOutput, calls=%fused_computation.clone.2 | convolution fusion | flops 125829120 | bytes 1589248 | tf_op jit(solution)/shard_map/while/body/eval_jaxpr/htc,htsc,hsc->hts/dot_general | solution.py:67
  557.3 68.5 %all-gather.23.cloned.1.call-done = f32[128,64,64]{2,1,0:T(8,128)} async-done(((f32[8,64,64]{2,1,0:T(8,128)}), f32[128,64,64]{2,1,0:T(8,128)}) %all-gather.23.cloned.1.call-update) | async-done | bytes 2097168 | tf_op jit(solution)/shard_map/all_gather | solution.py:17
  625.8 76.8 %all-gather.25.cloned.1.call-done = f32[128,64,64]{2,1,0:T(8,128)} async-done(((f32[8,64,64]{2,1,0:T(8,128)}), f32[128,64,64]{2,1,0:T(8,128)}) %all-gather.25.cloned.1.call-update) | async-done | bytes 2097168 | tf_op jit(solution)/shard_map/all_gather | solution.py:17
  702.6 43.6 %while.32 = (s32[]{:T(128)}, f32[8,64,64]{1,2,0:T(8,128)S(1)}, s32[]{:T(128)}, f32[16,8,64,64]{3,2,1,0:T(8,128)}, f32[16,8,64,64]{3,2,1,0:T(8,128)}, /*index=5*/s32[]{:T(128)}, s32[]{:T(128)}) while((s32[]{:T(128)}, f32[8,64,64]{1,2,0:T(8,128)S(1)}, s32[]{:T(128)}, f32[16,8,64,64]{3,2,1,0:T(8,128)}, f32[16,8,64,64]{3,2,1,0:T(8,128)}, ...), condition=%wide.region_8.9_spmd.clone, body=%wide.region_7.8_spmd.clone.sunk | while | flops 25296900 | bytes 1968227 | solution.py:27
  746.2 33.2 %all-gather.19.cloned.1.call-done = bf16[2048,1024]{1,0:T(8,128)(2,1)} async-done(((bf16[128,1024]{1,0:T(8,128)(2,1)}), bf16[2048,1024]{1,0:T(8,128)(2,1)}) %all-gather.19.cloned.1.call-update) | async-done | bytes 4194320 | tf_op jit(solution)/shard_map/all_gather | solution.py:150
  779.4 4.5 fusion.91
  783.9 72.3 %all-gather.17.cloned.1.call-done = bf16[2048,1024]{1,0:T(8,128)(2,1)} async-done(((bf16[128,1024]{1,0:T(8,128)(2,1)}), bf16[2048,1024]{1,0:T(8,128)(2,1)}) %all-gather.17.cloned.1.call-update) | async-done | bytes 4194320 | tf_op jit(solution)/shard_map/all_gather | solution.py:149
  865.3 6.0 fusion.146
  873.8 59.5 %all-gather.21.cloned.1.call-done = bf16[2048,1024]{1,0:T(8,128)(2,1)} async-done(((bf16[128,1024]{1,0:T(8,128)(2,1)}), bf16[2048,1024]{1,0:T(8,128)(2,1)}) %all-gather.21.cloned.1.call-update) | async-done | bytes 4194320 | tf_op jit(solution)/shard_map/all_gather | solution.py:241
  937.3 57.7 %all-gather.15.cloned.1.call-done = bf16[2048,512]{1,0:T(8,128)(2,1)} async-done(((bf16[128,512]{1,0:T(8,128)(2,1)}), bf16[2048,512]{1,0:T(8,128)(2,1)}) %all-gather.15.cloned.1.call-update) | async-done | bytes 2097168 | tf_op jit(solution)/shard_map/all_gather | solution.py:241
  998.4 18.4 %all-reduce.3.cloned.1.call-done = bf16[256,2048]{1,0:T(8,128)(2,1)} async-done(((bf16[256,2048]{1,0:T(8,128)(2,1)}), bf16[256,2048]{1,0:T(8,128)(2,1)}) %all-reduce.3.cloned.1.call-update) | async-done | bytes 1048592 | tf_op jit(solution)/shard_map/psum | solution.py:247
  (267 shorter events, 176.4 us)
Async XLA Ops:
  6.5 82.8 %all-gather.11.cloned.1.call-start = ((), (), s32[]{:S(2)}) async-start(), calls=%async_computation.1 | async-start | bytes 2228224 | tf_op jit(solution)/shard_map/all_gather | solution.py:147
  10.0 85.3 %all-to-all-start = ((bf16[16,128,512]{1,2,0:T(8,128)(2,1)}), bf16[16,128,512]{1,2,0:T(8,128)(2,1)S(1)}, u32[]{:S(2)}, u32[]{:S(2)}) async-start(bf16[16,128,512]{1,2,0:T(8,128)(2,1)} %stack.2), calls=%async_computation | async-start | bytes 4194304 | tf_op jit(solution)/shard_map/all_to_all | solution.py:145
  18.5 133.0 %all-gather.13.cloned.1.call-start = ((), (), s32[]{:S(2)}) async-start(), calls=%async_computation.2 | async-start | bytes 2228224 | tf_op jit(solution)/shard_map/all_gather | solution.py:148
  19.3 606.5 %all-gather.23.cloned.1.call-start = ((), (), s32[]{:S(2)}) async-start(), calls=%async_computation.8 | async-start | bytes 4456448 | tf_op jit(solution)/shard_map/all_gather | solution.py:17
  98.0 57.5 %copy-start.7 = (bf16[256,2048]{1,0:T(8,128)(2,1)S(1)}, bf16[256,2048]{1,0:T(8,128)(2,1)}, u32[]{:S(2)}) copy-start(bf16[256,2048]{1,0:T(8,128)(2,1)} %fusion.88) | copy-start | bytes 3145732
  102.1 56.6 %copy-start.9 = (f32[2,128,8,64]{1,0,3,2:T(2,128)S(1)}, f32[2,128,8,64]{1,0,3,2:T(2,128)}, u32[]{:S(2)}) copy-start(f32[2,128,8,64]{1,0,3,2:T(2,128)} %reshape.138) | copy-start | bytes 1572868
  191.8 33.9 %copy-start.2 = (f32[8,128,64]{2,1,0:T(8,128)}, f32[8,128,64]{2,1,0:T(8,128)S(1)}, u32[]{:S(2)}) copy-start(f32[8,128,64]{2,1,0:T(8,128)S(1)} %copy.255) | copy-start | bytes 786436 | tf_op jit(solution)/shard_map/while
  273.8 34.2 %copy-start.4 = (f32[8,128,64]{2,1,0:T(8,128)S(1)}, f32[8,128,64]{2,1,0:T(8,128)}, u32[]{:S(2)}) copy-start(f32[8,128,64]{2,1,0:T(8,128)} %copy-done.2) | copy-start | bytes 786436 | tf_op jit(solution)/shard_map/while
  273.8 34.2 %copy-start.6 = (f32[8,128,64,1]{2,3,1,0:T(1,128)S(1)}, f32[8,128,64,1]{2,3,1,0:T(1,128)}, u32[]{:S(2)}) copy-start(f32[8,128,64,1]{2,3,1,0:T(1,128)} %copy.256) | copy-start | bytes 786436 | tf_op jit(solution)/shard_map/while
  464.4 34.2 %copy-start.4 = (f32[8,128,64]{2,1,0:T(8,128)S(1)}, f32[8,128,64]{2,1,0:T(8,128)}, u32[]{:S(2)}) copy-start(f32[8,128,64]{2,1,0:T(8,128)} %copy-done.2) | copy-start | bytes 786436 | tf_op jit(solution)/shard_map/while
  464.4 34.2 %copy-start.6 = (f32[8,128,64,1]{2,3,1,0:T(1,128)S(1)}, f32[8,128,64,1]{2,3,1,0:T(1,128)}, u32[]{:S(2)}) copy-start(f32[8,128,64,1]{2,3,1,0:T(1,128)} %copy.256) | copy-start | bytes 786436 | tf_op jit(solution)/shard_map/while
  551.2 151.4 %all-gather.25.cloned.1.call-start = ((), (), s32[]{:S(2)}) async-start(), calls=%async_computation.9 | async-start | bytes 4456448 | tf_op jit(solution)/shard_map/all_gather | solution.py:17
  552.1 227.3 %all-gather.19.cloned.1.call-start = ((), (), s32[]{:S(2)}) async-start(), calls=%async_computation.5 | async-start | bytes 4456448 | tf_op jit(solution)/shard_map/all_gather | solution.py:150
  552.7 303.6 %all-gather.17.cloned.1.call-start = ((), (), s32[]{:S(2)}) async-start(), calls=%async_computation.4 | async-start | bytes 4456448 | tf_op jit(solution)/shard_map/all_gather | solution.py:149
  553.3 380.0 %all-gather.21.cloned.1.call-start = ((), (), s32[]{:S(2)}) async-start(), calls=%async_computation.6 | async-start | bytes 4456448 | tf_op jit(solution)/shard_map/all_gather | solution.py:241
  554.1 441.0 %all-gather.15.cloned.1.call-start = ((), (), s32[]{:S(2)}) async-start(), calls=%async_computation.3 | async-start | bytes 2228224 | tf_op jit(solution)/shard_map/all_gather | solution.py:241
  554.8 462.0 %all-reduce.3.cloned.1.call-start = ((), (), s32[]{:S(2)}) async-start(), calls=%async_computation.7 | async-start | bytes 2097152 | tf_op jit(solution)/shard_map/psum | solution.py:247
  702.6 76.8 %copy-start.8 = (bf16[256,2048]{1,0:T(8,128)(2,1)S(1)}, bf16[256,2048]{1,0:T(8,128)(2,1)}, u32[]{:S(2)}) copy-start(bf16[256,2048]{1,0:T(8,128)(2,1)} %fusion.88) | copy-start | bytes 3145732
  783.9 79.5 %copy-start.10 = (f32[2,8,128,64]{2,3,0,1:T(8,128)S(1)}, f32[2,8,128,64]{2,3,0,1:T(8,128)}, u32[]{:S(2)}) copy-start(f32[2,8,128,64]{2,3,0,1:T(8,128)} %get-tuple-element.159) | copy-start | bytes 1572868
  783.9 79.5 %copy-start.11 = (f32[2,8,128,64]{2,3,0,1:T(8,128)S(1)}, f32[2,8,128,64]{2,3,0,1:T(8,128)}, u32[]{:S(2)}) copy-start(f32[2,8,128,64]{2,3,0,1:T(8,128)} %get-tuple-element.163) | copy-start | bytes 1572868
  783.9 80.7 %copy-start.15 = (f32[512]{0:T(512)S(1)}, f32[512]{0:T(512)}, u32[]{:S(2)}) copy-start(f32[512]{0:T(512)} %param.39) | copy-start | bytes 6148
  860.0 73.3 %copy-start.17 = (f32[1024]{0:T(1024)S(1)}, f32[1024]{0:T(1024)}, u32[]{:S(2)}) copy-start(f32[1024]{0:T(1024)} %param.41) | copy-start | bytes 12292
  860.1 5.2 collective-permute-start
  933.3 85.8 %copy-start.1 = (bf16[2048,128]{1,0:T(8,128)(2,1)S(1)}, bf16[2048,128]{1,0:T(8,128)(2,1)}, u32[]{:S(2)}) copy-start(bf16[2048,128]{1,0:T(8,128)(2,1)} %param.35) | copy-start | bytes 1572868
  (12 other events, 119.2 us)
Sparse Core Ops, SparseCore 0:
  10.1 79.1 all-gather.10
  92.1 59.3 all-gather.12
  551.3 74.3 all-gather.22
  628.4 74.1 all-gather.24
  705.2 74.1 all-gather.18
  782.1 74.1 all-gather.16
  859.1 74.1 all-gather.20
  936.1 58.9 all-gather.14
  998.5 18.1 all-reduce.2
